TPU v7x, 32 devices: a whole 2x2x4 slice. The times are simulated.
32 devices in a mesh: sp: 8 (over z, x), tp: 4 (over y, core).
Axes of the slice: x: 2, y: 2, z: 4, core: 2. Of those that a mesh axis runs over, the one named last changes fastest.
Arguments:
- resid: bfloat16 [2048, 2048], P('sp'), may hold values from -6 to 6
- query_one: bfloat16 [2048, 1024], P('sp', 'tp'), may hold values from -400 to 400
- query_two: bfloat16 [2048, 1024], P('sp', 'tp'), may hold values from -400 to 400
- key_one: bfloat16 [2048, 1024], P('sp', 'tp'), may hold values from -8 to 8
- key_two: bfloat16 [2048, 1024], P('sp', 'tp'), may hold values from -8 to 8
- values: bfloat16 [2048, 2048], P('sp', 'tp'), may hold values from -6 to 6
- documents: int32 [2048], P('sp'), may hold values from 0 to 1, never falling along the last dimension, each value on 1 to 1280 neighbouring positions
- mix_lambda: float32 [16], P('tp'), may hold values from 0.3 to 0.8
- head_gain: float32 [128], replicated, may hold values from 0.1 to 1.9
- out_weight: bfloat16 [2048, 2048], P('tp'), may hold values from -0.125 to 0.125
- ffn_gain: float32 [2048], replicated, may hold values from 0.1 to 1.9
- routes: int32 [2048, 4], P('sp'), may hold values from 0 to 31, all different within a row; in each aligned block of 256 rows (0 to 255, 256 to 511, ...) at most 64 rows name the same one
- route_weight: float32 [2048, 4], P('sp'), may hold values from 0.2 to 0.9
- expert_gate: bfloat16 [32, 2048, 512], P(('sp', 'tp')), may hold values from -0.125 to 0.125
- expert_up: bfloat16 [32, 2048, 512], P(('sp', 'tp')), may hold values from -0.125 to 0.125
- expert_down: bfloat16 [32, 512, 2048], P(('sp', 'tp')), may hold values from -0.25 to 0.25
- shared_gate: bfloat16 [2048, 512], P(None, 'tp'), may hold values from -0.125 to 0.125
- shared_up: bfloat16 [2048, 512], P(None, 'tp'), may hold values from -0.125 to 0.125
- shared_down: bfloat16 [512, 2048], P('tp'), may hold values from -0.25 to 0.25
Outputs:
- layer_out: bfloat16 [2048, 2048], P(('sp', 'tp'))
Inputs may be any that keep to these rules, and one draw needn't show every extreme that they name: `documents`: document numbers never fall along the positions; each document has 1 to 1280 positions and one has exactly 1280. `routes`: A row names 4 different experts. In each aligned block of 256 rows no expert is named by more than 64 rows, a bound that some block reaches.
All inputs are finite; a program needn't handle non-finite values.
Results may differ from a plain program's by a relative error of at most 0.018.
Values may be sent and summed in bfloat16 or wider, within the bound.
A program may use at most 128 MiB of HBM per device.

v0:
```python
import jax
import jax.numpy as jnp
from jax import lax
from jax.sharding import PartitionSpec as P

NEG_FILL = -1e30
HEAD_SCALE = 0.8


def rms_scale(values_in, eps_value):
    return lax.rsqrt(jnp.mean(values_in * values_in, axis=-1, keepdims=True) + eps_value)


def local(
    resid,
    query_one,
    query_two,
    key_one,
    key_two,
    values,
    documents,
    mix_lambda,
    head_gain,
    out_weight,
    ffn_gain,
    routes,
    route_weight,
    expert_gate,
    expert_up,
    expert_down,
    shared_gate,
    shared_up,
    shared_down,
):
    tok_rows = query_one.shape[0]
    head_count = mix_lambda.shape[0]
    head_width = query_one.shape[1] // head_count
    value_width = values.shape[1] // head_count
    model_width = resid.shape[1]
    score_scale = head_width ** (-0.5)
    seq_size = lax.axis_size("sp")
    tp_size = lax.axis_size("tp")
    query_pos = lax.axis_index("sp") * tok_rows + jnp.arange(tok_rows, dtype=jnp.int32)
    query_first = query_one.reshape(tok_rows, head_count, head_width)
    query_second = query_two.reshape(tok_rows, head_count, head_width)
    lambda_col = mix_lambda[:, None, None]
    first_doc = documents[0]
    last_pos = query_pos[tok_rows - 1]

    def masks(key_docs):
        key_pos = jnp.arange(key_docs.shape[0], dtype=jnp.int32)
        return (
            (key_pos[None, :] <= query_pos[:, None]) & (key_docs[None, :] == documents[:, None])
        )[None]

    def needed(key_docs, offset):
        return (offset <= last_pos) & (jnp.max(key_docs) >= first_doc)

    def scores(query_block, key_block):
        keyed = key_block.reshape(key_block.shape[0], head_count, head_width)
        return (
            jnp.einsum("qhd,khd->hqk", query_block, keyed, preferred_element_type=jnp.float32)
            * score_scale
        )

    empty_max = jnp.full((head_count, tok_rows), NEG_FILL, jnp.float32)
    empty_sum = jnp.zeros((head_count, tok_rows), jnp.float32)
    stats_init = ((empty_max, empty_sum), (empty_max, empty_sum))
    value_init = jnp.zeros((head_count, tok_rows, value_width), jnp.float32)
    key_first = lax.all_gather(key_one, "sp", axis=0, tiled=True)
    key_second = lax.all_gather(key_two, "sp", axis=0, tiled=True)
    key_docs = lax.all_gather(documents, "sp", axis=0, tiled=True)

    def stats_update(current):
        allowed = masks(key_docs)
        result = []
        for query_block, key_block, (top_now, sum_now) in (
            (query_first, key_first, current[0]),
            (query_second, key_second, current[1]),
        ):
            masked = jnp.where(allowed, scores(query_block, key_block), NEG_FILL)
            top_next = jnp.maximum(top_now, jnp.max(masked, axis=-1))
            fresh = jnp.where(allowed, jnp.exp(masked - top_next[:, :, None]), 0.0)
            result.append((top_next, jnp.sum(fresh, axis=-1)))
        return tuple(result)

    def stats_keep(current):
        return current

    soft_stats = lax.cond(needed(key_docs, jnp.int32(0)), stats_update, stats_keep, stats_init)
    apply_key_first = lax.all_gather(key_one, "sp", axis=0, tiled=True)
    apply_key_second = lax.all_gather(key_two, "sp", axis=0, tiled=True)
    value_block = lax.all_gather(values, "sp", axis=0, tiled=True)
    apply_key_docs = lax.all_gather(documents, "sp", axis=0, tiled=True)

    def apply_update(current):
        allowed = masks(apply_key_docs)
        probs = []
        for query_block, key_block, (top_all, sum_all) in (
            (query_first, apply_key_first, soft_stats[0]),
            (query_second, apply_key_second, soft_stats[1]),
        ):
            raw = scores(query_block, key_block)
            probs.append(
                jnp.where(allowed, jnp.exp(raw - top_all[:, :, None]), 0.0) / sum_all[:, :, None]
            )
        weights = (probs[0] - lambda_col * probs[1]).astype(jnp.bfloat16)
        valued = value_block.reshape(value_block.shape[0], head_count, value_width)
        return current + jnp.einsum(
            "hqk,khv->hqv", weights, valued, preferred_element_type=jnp.float32
        )

    def apply_keep(current):
        return current

    head_out = lax.cond(needed(apply_key_docs, jnp.int32(0)), apply_update, apply_keep, value_init)
    normed_heads = (head_out * rms_scale(head_out, 1e-05) * head_gain * HEAD_SCALE).astype(
        jnp.bfloat16
    )
    attn_rows = normed_heads.transpose(1, 0, 2).reshape(tok_rows, head_count * value_width)
    share_rows = tok_rows // tp_size
    own_start = lax.axis_index("tp") * share_rows
    proj_term = jnp.dot(attn_rows, out_weight, preferred_element_type=jnp.float32)
    projected = lax.psum(proj_term.astype(jnp.bfloat16), "tp").astype(jnp.float32)
    mixed_all = resid.astype(jnp.float32) + projected
    normed_all = (mixed_all * rms_scale(mixed_all, 1e-06) * ffn_gain).astype(jnp.bfloat16)
    mixed_own = lax.dynamic_slice_in_dim(mixed_all, own_start, share_rows, 0)
    route_slots = routes.shape[1]
    capacity = max(2, 2 * tok_rows * route_slots // (seq_size * tp_size))
    assign_total = tok_rows * route_slots
    flat_expert = routes.reshape(assign_total)
    flat_weight = route_weight.reshape(assign_total)
    assign_token = jnp.arange(assign_total, dtype=jnp.int32) // route_slots
    is_mine = flat_expert % tp_size == lax.axis_index("tp")
    target = flat_expert // tp_size
    one_hot = (
        (target[:, None] == jnp.arange(seq_size, dtype=jnp.int32)[None, :]) & is_mine[:, None]
    ).astype(jnp.int32)
    slot_rank = jnp.sum(jnp.cumsum(one_hot, axis=0) * one_hot, axis=1) - 1
    slot_id = jnp.where(is_mine, target * capacity + slot_rank, -1)
    slot_total = seq_size * capacity
    matches = slot_id[None, :] == jnp.arange(slot_total, dtype=jnp.int32)[:, None]
    slot_token = jnp.sum(jnp.where(matches, assign_token[None, :], 0), axis=1)
    slot_live = jnp.any(matches, axis=1)
    outgoing = jnp.where(
        slot_live[:, None], normed_all[slot_token], jnp.zeros((), jnp.bfloat16)
    ).reshape(seq_size, capacity, model_width)
    arrived = lax.all_to_all(outgoing, "sp", split_axis=0, concat_axis=0, tiled=True)
    item_count = arrived.shape[1]
    flat_rows = arrived.reshape(seq_size * item_count, model_width)
    gate_part = jnp.dot(flat_rows, expert_gate[0], preferred_element_type=jnp.float32)
    up_part = jnp.dot(flat_rows, expert_up[0], preferred_element_type=jnp.float32)
    hidden = (jax.nn.silu(gate_part) * up_part).astype(jnp.bfloat16)
    result = jnp.dot(hidden, expert_down[0], preferred_element_type=jnp.float32).astype(
        jnp.bfloat16
    )
    returned = lax.all_to_all(
        result.reshape(seq_size, item_count, model_width),
        "sp",
        split_axis=0,
        concat_axis=0,
        tiled=True,
    )
    returned_flat = returned.reshape(slot_total, model_width)
    picked = returned_flat[jnp.maximum(slot_id, 0)].astype(jnp.float32)
    picked_weight = jnp.where(is_mine, flat_weight, 0.0)
    routed = jnp.sum(
        (picked * picked_weight[:, None]).reshape(tok_rows, route_slots, model_width), axis=1
    )
    shared_act = (
        jax.nn.silu(jnp.dot(normed_all, shared_gate, preferred_element_type=jnp.float32))
        * jnp.dot(normed_all, shared_up, preferred_element_type=jnp.float32)
    ).astype(jnp.bfloat16)
    shared_out = jnp.dot(shared_act, shared_down, preferred_element_type=jnp.float32)
    ffn_own = lax.psum_scatter(
        (routed + shared_out).astype(jnp.bfloat16), "tp", scatter_dimension=0, tiled=True
    ).astype(jnp.float32)
    return (mixed_own + ffn_own).astype(jnp.bfloat16)


def solution(mesh):
    placed = (
        P("sp", None),
        P("sp", "tp"),
        P("sp", "tp"),
        P("sp", "tp"),
        P("sp", "tp"),
        P("sp", "tp"),
        P("sp"),
        P("tp"),
        P(),
        P("tp", None),
        P(),
        P("sp", None),
        P("sp", None),
        P(("sp", "tp"), None, None),
        P(("sp", "tp"), None, None),
        P(("sp", "tp"), None, None),
        P(None, "tp"),
        P(None, "tp"),
        P("tp", None),
    )
    return jax.shard_map(
        local, mesh=mesh, in_specs=placed, out_specs=P(("sp", "tp"), None), check_vma=False
    )
```

profile of v0, /device:TPU:0, one launch (start us, length us, event | category | flops | bytes accessed | tf_op | source)
XLA Modules:
  0.0 388.5 jit_solution(5894218725486632129)
XLA Ops:
  15.9 22.3 %all-gather = s32[8,1,256]{2,1,0:T(1,128)S(1)} all-gather(s32[1,1,256]{2,1,0:T(1,128)S(1)} %bitcast.92), channel_id=1, replica_groups=mesh['sp'=8,'tp'=4] {'sp'}, dimensions={0}, use_global_device_ids=true | all-gather | bytes 9216 | tf_op jit(solution)/shard_map/all_gather | solution.py:94
  42.9 8.6 %all-gather.5.cloned.1.call-done = bf16[2048,256]{0,1:T(8,128)(2,1)} async-done(((bf16[256,256]{0,1:T(8,128)(2,1)}), bf16[2048,256]{0,1:T(8,128)(2,1)}) %all-gather.5.cloned.1.call-update) | async-done | bytes 1048592 | tf_op jit(solution)/shard_map/all_gather | solution.py:91
  51.6 40.5 %all-gather.7.cloned.1.call-done = bf16[2048,256]{0,1:T(8,128)(2,1)} async-done(((bf16[256,256]{0,1:T(8,128)(2,1)}), bf16[2048,256]{0,1:T(8,128)(2,1)}) %all-gather.7.cloned.1.call-update) | async-done | bytes 1048592 | tf_op jit(solution)/shard_map/all_gather | solution.py:71
  92.0 12.4 %conditional.2 = (f32[4,256]{1,0:T(4,128)}, f32[4,256]{1,0:T(4,128)S(1)}, f32[4,256]{1,0:T(4,128)}, f32[4,256]{1,0:T(4,128)S(1)}) conditional(s32[]{:T(128)} %convert_element_type.53, () %tuple.24, (s32[256]{0:T(256)S(1)}, s32[2048]{0:T(1024)S(1)}, s32[256]{0:T(256)S(1)}, bf16[2048,256]{0,1:T(8,128)(2,1)}, bf16[256,4,64]{0,2,1:T(8,128)(2,1)S(1)}, ...), branch_computations={%region_1.0_spmd, %region_2.7_spmd} | conditional | flops 571996160 | bytes 50120764 | solution.py:90
  92.0 2.6 fusion.55
  95.2 3.1 fusion.1
  98.9 5.5 %select_reduce_fusion = (f32[4,256]{1,0:T(4,128)S(1)}, f32[4,256]{1,0:T(4,128)S(1)}) fusion(f32[4,256,2048]{2,1,0:T(8,128)S(1)} %get-tuple-element.106, f32[4,256]{1,0:T(4,128)} %get-tuple-element.122, pred[256,2048]{1,0:T(8,128)(4,1)S(1)} %fusion.2, f32[4,256]{1,0:T(4,128)} %get-tuple-element.120, f32[4,256,2048]{2,1,0:T(8,128)S(1)} %fusion.55), kind=kLoop, calls=%fused_computation.2 | loop fusion | flops 20969472 | bytes 17317888 | tf_op jit(solution)/shard_map/cond/branch_1_fun/reduce_sum | solution.py:84
  104.4 39.0 %all-gather.9.cloned.1.call-done = bf16[2048,512]{0,1:T(8,128)(2,1)} async-done(((bf16[256,512]{0,1:T(8,128)(2,1)}), bf16[2048,512]{0,1:T(8,128)(2,1)}) %all-gather.9.cloned.1.call-update) | async-done | bytes 2097168 | tf_op jit(solution)/shard_map/all_gather | solution.py:93
  143.5 16.7 %conditional.3 = (f32[4,256,128]{1,2,0:T(8,128)S(1)}, f32[4,256,1]{1,0,2:T(4,128)S(1)}) conditional(s32[]{:T(128)} %convert_element_type.53, () %tuple.23, (s32[256]{0:T(256)S(1)}, s32[2048]{0:T(1024)S(1)}, s32[256]{0:T(256)S(1)}, bf16[2048,256]{0,1:T(8,128)(2,1)}, bf16[256,4,64]{0,2,1:T(8,128)(2,1)S(1)}, /*index=5*/f32[4,256]{1,0:T(4,128)}, ...), branch_computations={%region_7.8_spmd, %region_8.0_spmd} | conditional | flops 1098644480 | bytes 22837280 | solution.py:116
  143.5 5.7 %fusion.56 = f32[4,256,2048]{2,1,0:T(8,128)} fusion(bf16[256,4,64]{0,2,1:T(8,128)(2,1)S(1)} %get-tuple-element.58, bf16[2048,4,64]{0,2,1:T(8,128)(2,1)} %bitcast.75), kind=kOutput, calls=%fused_computation.113 | convolution fusion | flops 268435456 | bytes 9568256 | tf_op jit(solution)/shard_map/cond/branch_1_fun/qhd,khd->hqk/dot_general | solution.py:62
  150.6 9.6 %multiply_reduce_fusion = (f32[4,256]{1,0:T(4,128)S(1)}, f32[4,256,128]{1,2,0:T(8,128)S(1)}) fusion(bf16[2048,4,128]{0,2,1:T(8,128)(2,1)} %bitcast.95, f32[4,256,2048]{2,1,0:T(8,128)} %fusion.56, bf16[256,4,64]{0,2,1:T(8,128)(2,1)S(1)} %get-tuple-element.63, bf16[2048,4,64]{0,2,1:T(8,128)(2,1)} %bitcast.82, f32[4,256]{1,0:T(4,128)S(1)} %get-tuple-element.66, ...), kind=kOutput, calls=%fused_computation.21 | convolution fusion | flops 828636160 | bytes 12734480 | tf_op jit(solution)/shard_map/cond/branch_1_fun/hqk,khv->hqv/dot_general | solution.py:109
  160.4 3.4 convolution_convert_fusion.1
  164.6 33.9 %all-reduce.2.cloned.1.call-done = bf16[256,2048]{1,0:T(8,128)(2,1)} async-done(((bf16[256,2048]{1,0:T(8,128)(2,1)}), bf16[256,2048]{1,0:T(8,128)(2,1)}) %all-reduce.2.cloned.1.call-update) | async-done | bytes 1048592 | tf_op jit(solution)/shard_map/psum | solution.py:124
  198.5 3.1 convert_add_fusion
  202.2 3.3 gather_fusion
  207.3 53.2 %all_to_all.10 = bf16[8,64,2048]{2,1,0:T(8,128)(2,1)S(1)} all-to-all(bf16[8,64,2048]{2,1,0:T(8,128)(2,1)S(1)} %broadcast_select_fusion), channel_id=1, replica_groups=mesh['sp'=8,'tp'=4] {'sp'}, dimensions={0} | all-to-all | bytes 4194304 | tf_op jit(solution)/shard_map/all_to_all | solution.py:148
  264.1 6.3 %convolution_convert_fusion = bf16[512,2048]{1,0:T(8,128)(2,1)} fusion(bf16[1,512,2048]{2,1,0:T(8,128)(2,1)S(1)} %copy-done, bf16[512,2048]{1,0:T(8,128)(2,1)} %bitcast.78, bf16[1,2048,512]{2,1,0:T(8,128)(2,1)} %param.37, f32[512,512]{1,0:T(8,128)} %fusion.16), kind=kOutput, calls=%fused_computation.25 | convolution fusion | flops 2150105088 | bytes 9437184 | tf_op jit(solution)/shard_map/dot_general | solution.py:154
  270.3 4.5 %all-to-all-start.1 = ((bf16[8,64,2048]{2,1,0:T(8,128)(2,1)}), bf16[8,64,2048]{2,1,0:T(8,128)(2,1)}, u32[]{:S(2)}, u32[]{:S(2)}) async-start(bf16[8,64,2048]{2,1,0:T(8,128)(2,1)} %bitcast.76), calls=%async_computation.1 | async-start | bytes 4194304 | tf_op jit(solution)/shard_map/all_to_all | solution.py:157
  276.7 45.4 %all-to-all-done.1 = bf16[8,64,2048]{2,1,0:T(8,128)(2,1)} async-done(((bf16[8,64,2048]{2,1,0:T(8,128)(2,1)}), bf16[8,64,2048]{2,1,0:T(8,128)(2,1)}, u32[]{:S(2)}, u32[]{:S(2)}) %all-to-all-start.1) | async-done | bytes 2097184 | tf_op jit(solution)/shard_map/all_to_all | solution.py:157
  322.1 10.7 %gather_fusion.1 = bf16[1024,2048]{1,0:T(8,128)(2,1)} fusion(bf16[512,2048]{1,0:T(8,128)(2,1)} %bitcast.24, s32[1024]{0:T(1024)S(1)} %broadcast_clamp_fusion), kind=kCustom, calls=%fused_computation.1 | custom fusion | bytes 8392704 | tf_op jit(solution)/shard_map/gather | solution.py:165
  332.8 8.3 %reshape.441 = f32[256,4,2048]{2,1,0:T(4,128)} reshape(bf16[1024,2048]{1,0:T(8,128)(2,1)} %gather_fusion.1) | data formatting | bytes 12582912 | tf_op jit(solution)/shard_map/convert_element_type | solution.py:165
  341.1 11.4 %multiply_reduce_fusion.1 = f32[256,2048]{1,0:T(8,128)} fusion(f32[256,4,2048]{2,1,0:T(4,128)} %reshape.441, f32[256,4]{1,0:T(8,128)S(1)} %copy.55), kind=kLoop, calls=%fused_computation.24 | loop fusion | flops 3670016 | bytes 10489856 | tf_op jit(solution)/shard_map/reduce_sum | solution.py:167
  352.5 3.7 fusion.12
  356.2 23.9 %reduce-scatter.2.cloned.1.call-done = bf16[64,2048]{1,0:T(8,128)(2,1)} async-done(((bf16[256,2048]{1,0:T(8,128)(2,1)}), bf16[64,2048]{1,0:T(8,128)(2,1)}) %reduce-scatter.2.cloned.1.call-update) | async-done | bytes 262160 | tf_op jit(solution)/shard_map/reduce_scatter | solution.py:175
  (82 shorter events, 25.2 us)
Async XLA Ops:
  6.5 257.5 %copy-start = (bf16[1,512,2048]{2,1,0:T(8,128)(2,1)S(1)}, bf16[1,512,2048]{2,1,0:T(8,128)(2,1)}, u32[]{:S(2)}) copy-start(bf16[1,512,2048]{2,1,0:T(8,128)(2,1)} %param.38) | copy-start | bytes 6291460
  6.5 7.6 %copy-start.6 = (bf16[256,256]{1,0:T(8,128)(2,1)S(1)}, bf16[256,256]{1,0:T(8,128)(2,1)}, u32[]{:S(2)}) copy-start(bf16[256,256]{1,0:T(8,128)(2,1)} %param.25) | copy-start | bytes 393220
  6.5 8.3 %copy-start.8 = (s32[256]{0:T(256)S(1)}, s32[256]{0:T(256)}, u32[]{:S(2)}) copy-start(s32[256]{0:T(256)} %param.29) | copy-start | bytes 3076
  6.5 45.0 %all-gather.5.cloned.1.call-start = ((), (), s32[]{:S(2)}) async-start(), calls=%async_computation.3 | async-start | bytes 1179648 | tf_op jit(solution)/shard_map/all_gather | solution.py:91
  8.4 83.7 %all-gather.7.cloned.1.call-start = ((), (), s32[]{:S(2)}) async-start(), calls=%async_computation.4 | async-start | bytes 1179648 | tf_op jit(solution)/shard_map/all_gather | solution.py:71
  10.1 133.4 %all-gather.9.cloned.1.call-start = ((), (), s32[]{:S(2)}) async-start(), calls=%async_computation.5 | async-start | bytes 2359296 | tf_op jit(solution)/shard_map/all_gather | solution.py:93
  12.0 186.5 %all-reduce.2.cloned.1.call-start = ((), (), s32[]{:S(2)}) async-start(), calls=%async_computation.6 | async-start | bytes 2097152 | tf_op jit(solution)/shard_map/psum | solution.py:124
  92.0 51.5 %copy-start.13 = (f32[4]{0:T(128)S(1)}, f32[4]{0:T(128)}, u32[]{:S(2)}) copy-start(f32[4]{0:T(128)} %param.30) | copy-start | bytes 52
  92.0 3.2 copy-start.5
  143.5 16.8 %copy-start.11 = (f32[128]{0:T(128)S(1)}, f32[128]{0:T(128)}, u32[]{:S(2)}) copy-start(f32[128]{0:T(128)} %param.31) | copy-start | bytes 1540
  160.4 38.1 %copy-start.1 = (bf16[256,2048]{1,0:T(8,128)(2,1)S(1)}, bf16[256,2048]{1,0:T(8,128)(2,1)}, u32[]{:S(2)}) copy-start(bf16[256,2048]{1,0:T(8,128)(2,1)} %param.23) | copy-start | bytes 3145732
  164.6 37.0 %copy-start.9 = (f32[2048]{0:T(1024)S(1)}, f32[2048]{0:T(1024)}, u32[]{:S(2)}) copy-start(f32[2048]{0:T(1024)} %param.33) | copy-start | bytes 24580
  198.5 3.1 copy-start.2
  198.5 3.1 copy-start.3
  207.3 54.5 %copy-start.12 = (bf16[1,2048,512]{2,1,0:T(8,128)(2,1)S(1)}, bf16[1,2048,512]{2,1,0:T(8,128)(2,1)}, u32[]{:S(2)}) copy-start(bf16[1,2048,512]{2,1,0:T(8,128)(2,1)} %param.36) | copy-start | bytes 6291460
  260.5 1.3 copy-start.4
  270.3 4.7 %copy-start.7 = (s32[256,4]{0,1:T(4,128)S(1)}, s32[256,4]{0,1:T(4,128)}, u32[]{:S(2)}) copy-start(s32[256,4]{0,1:T(4,128)} %param.34) | copy-start | bytes 12292
  270.3 4.7 %copy-start.10 = (f32[256,4]{0,1:T(4,128)S(1)}, f32[256,4]{0,1:T(4,128)}, u32[]{:S(2)}) copy-start(f32[256,4]{0,1:T(4,128)} %param.35) | copy-start | bytes 12292
  270.3 51.7 %all-to-all-start.1 = ((bf16[8,64,2048]{2,1,0:T(8,128)(2,1)}), bf16[8,64,2048]{2,1,0:T(8,128)(2,1)}, u32[]{:S(2)}, u32[]{:S(2)}) async-start(bf16[8,64,2048]{2,1,0:T(8,128)(2,1)} %bitcast.76), calls=%async_computation.1 | async-start | bytes 4194304 | tf_op jit(solution)/shard_map/all_to_all | solution.py:157
  274.8 105.3 %reduce-scatter.2.cloned.1.call-start = ((), (), s32[]{:S(2)}) async-start(), calls=%async_computation.7 | async-start | bytes 1310720 | tf_op jit(solution)/shard_map/reduce_scatter | solution.py:175
Sparse Core Ops, SparseCore 0:
  9.4 42.1 all-gather.4
  53.6 38.3 all-gather.6
  94.1 49.3 all-gather.8
  164.0 34.4 all-reduce.1
  356.3 23.7 reduce-scatter.1
where the time goes:
time: 389 us
  waiting for transfers between devices  191 us (49%)
  blocking collectives  75.5 us (19%)
  matrix products  38.2 us (10%)
  local copies, waits for them, and re-layouts  32.8 us (8%)
  other arithmetic  30.8 us (8%)
  between operations  15.1 us (4%)
  starting transfers between devices  4.67 us (1%)
    all_to_all x1, blocking collectives, local(): lax.all_to_all(outgoing, 'sp', split_axis=0, concat_axis=0, tiled=True)  53.2 us
    all_to_all x1, waiting for transfers between devices, local(): lax.all_to_all(result.reshape(seq_size, item_count, model_width), 'sp', s...  45.4 us
    all_gather x1, waiting for transfers between devices, local(): key_second = lax.all_gather(key_two, 'sp', axis=0, tiled=True)  40.5 us
    all_gather x1, waiting for transfers between devices, local(): value_block = lax.all_gather(values, 'sp', axis=0, tiled=True)  39 us
    psum x1, waiting for transfers between devices, local(): lax.psum(proj_term.astype(jnp.bfloat16), 'tp').astype(jnp.float32)  33.9 us
    reduce_scatter x1, waiting for transfers between devices, local(): lax.psum_scatter((routed + shared_out).astype(jnp.bfloat16), 'tp', scatte...  23.9 us
    all_gather x1, blocking collectives, local(): apply_key_docs = lax.all_gather(documents, 'sp', axis=0, tiled=True)  22.3 us
    dot_general x3, matrix products, scores(): jnp.einsum('qhd,khd->hqk', query_block, keyed, preferred_element_type=jnp...  11.5 us
  transfers between devices with their start and end apart: 6, of which 6 were waited for; matrix products, arithmetic and copies ran while one was open for 6% of the time, Pallas kernels for 0%

commit v1 on v0

--- a/solution.py
+++ b/solution.py
@@ -5,6 +5,19 @@
 
 NEG_FILL = -1e30
 HEAD_SCALE = 0.8
+
+
+def gather_around(x, axis, dim):
+    ways = lax.axis_size(axis)
+    up = [(d, (d + 1) % ways) for d in range(ways)]
+    down = [(d, (d - 1) % ways) for d in range(ways)]
+    earlier, later = ([x], [x])
+    for _ in range(ways // 2):
+        earlier.append(lax.ppermute(earlier[-1], axis, up))
+    for _ in range((ways - 1) // 2):
+        later.append(lax.ppermute(later[-1], axis, down))
+    line = jnp.concatenate([*earlier[::-1], *later[1:]], axis=dim)
+    return jnp.roll(line, (lax.axis_index(axis) - ways // 2) * x.shape[dim], axis=dim)
 
 
 def rms_scale(values_in, eps_value):
@@ -90,7 +103,7 @@
     soft_stats = lax.cond(needed(key_docs, jnp.int32(0)), stats_update, stats_keep, stats_init)
     apply_key_first = lax.all_gather(key_one, "sp", axis=0, tiled=True)
     apply_key_second = lax.all_gather(key_two, "sp", axis=0, tiled=True)
-    value_block = lax.all_gather(values, "sp", axis=0, tiled=True)
+    value_block = gather_around(values, "sp", 0)
     apply_key_docs = lax.all_gather(documents, "sp", axis=0, tiled=True)
 
     def apply_update(current):

time: 389 us -> 375 us (0.964)
  waiting for transfers between devices: 191 us -> 137 us
  local copies, waits for them, and re-layouts: 32.8 us -> 55.7 us
  starting transfers between devices: 4.67 us -> 22.2 us
    all_gather x1 -> x0, waiting for transfers between devices: 39 us -> none  [local(): value_block = lax.all_gather(values, 'sp', axis=0, tiled=True)]
    all_gather x1, waiting for transfers between devices: 40.5 us -> 6.67 us  [local(): key_second = lax.all_gather(key_two, 'sp', axis=0, tiled=True)]
    ppermute x0 -> x7, waiting for transfers between devices: none -> 26.4 us  [the longest x4 26.4 us: gather_around(): earlier.append(lax.ppermute(earlier[-1], axis, up))]
    ppermute x0 -> x7, starting transfers between devices: none -> 17.6 us  [the longest x3 9.52 us: gather_around(): later.append(lax.ppermute(later[-1], axis, down))]
    unnamed x32 -> x47, local copies, waits for them, and re-layouts: 8.52 us -> 25.6 us
    all_gather x1, waiting for transfers between devices: 8.64 us -> 0.01 us  [local(): apply_key_first = lax.all_gather(key_one, 'sp', axis=0, tiled=True)]
    dynamic_slice x0 -> x1, local copies, waits for them, and re-layouts: none -> 4.33 us  [gather_around(): jnp.roll(line, (lax.axis_index(axis) - ways // 2) * x.shape[dim], axis=dim)]
  transfers between devices with their start and end apart: 6 -> 12, of which waited for: 6 -> 7; matrix products, arithmetic and copies ran while one was open for 6% -> 9% of each run, Pallas kernels for 0% -> 0%
where the time goes in v1:
time: 375 us; the launch traced here: 374 us
  waiting for transfers between devices  137 us (37%)
  blocking collectives  71.7 us (19%)
  local copies, waits for them, and re-layouts  55.7 us (15%)
  matrix products  37.5 us (10%)
  other arithmetic  34.3 us (9%)
  starting transfers between devices  22.2 us (6%)
  between operations  15.2 us (4%)
    all_to_all x1, blocking collectives, local(): lax.all_to_all(outgoing, 'sp', split_axis=0, concat_axis=0, tiled=True)  53.1 us
    all_to_all x1, waiting for transfers between devices, local(): lax.all_to_all(result.reshape(seq_size, item_count, model_width), 'sp', s...  45.3 us
    psum x1, waiting for transfers between devices, local(): lax.psum(proj_term.astype(jnp.bfloat16), 'tp').astype(jnp.float32)  34.7 us
    ppermute x4, waiting for transfers between devices, gather_around(): earlier.append(lax.ppermute(earlier[-1], axis, up))  26.4 us
    unnamed x47, local copies, waits for them, and re-layouts  25.6 us
    reduce_scatter x1, waiting for transfers between devices, local(): lax.psum_scatter((routed + shared_out).astype(jnp.bfloat16), 'tp', scatte...  23.9 us
    all_gather x1, blocking collectives, local(): apply_key_docs = lax.all_gather(documents, 'sp', axis=0, tiled=True)  18.7 us
    reduce_sum x1, other arithmetic, local(): jnp.sum((picked * picked_weight[:, None]).reshape(tok_rows, route_slots,...  11.4 us
  transfers between devices with their start and end apart: 12, of which 7 were waited for; matrix products, arithmetic and copies ran while one was open for 9% of the time, Pallas kernels for 0%

profile of v1, /device:TPU:0, one launch (start us, length us, event | category | flops | bytes accessed | tf_op | source)
XLA Modules:
  0.0 373.9 jit_solution(313889155098211797)
XLA Ops:
  20.8 4.3 %collective-permute-done = bf16[256,512]{0,1:T(8,128)(2,1)S(1)} collective-permute-done((bf16[256,512]{0,1:T(8,128)(2,1)S(1)}, bf16[256,512]{0,1:T(8,128)(2,1)S(1)}, u32[]{:S(2)}, u32[]{:S(2)}) %collective-permute-start) | collective-permute-done | bytes 262176 | tf_op jit(solution)/shard_map/ppermute | solution.py:16
  28.1 10.8 %collective-permute-done.1 = bf16[256,512]{0,1:T(8,128)(2,1)S(1)} collective-permute-done((bf16[256,512]{0,1:T(8,128)(2,1)S(1)}, bf16[256,512]{0,1:T(8,128)(2,1)S(1)}, u32[]{:S(2)}, u32[]{:S(2)}) %collective-permute-start.1) | collective-permute-done | bytes 262176 | tf_op jit(solution)/shard_map/ppermute | solution.py:16
  39.5 4.7 %collective-permute-start.5 = (bf16[256,512]{0,1:T(8,128)(2,1)S(1)}, bf16[256,512]{0,1:T(8,128)(2,1)}, u32[]{:S(2)}, u32[]{:S(2)}) collective-permute-start(bf16[256,512]{0,1:T(8,128)(2,1)S(1)} %collective-permute-done.4), channel_id=1, source_target_pairs={{0,28},{4,0},{8,4},{12,8},{16,12},{20,16},{24,20},{28,24},{1,29},{... | collective-permute-start | bytes 786440 | tf_op jit(solution)/shard_map/ppermute | solution.py:18
  44.3 11.3 %collective-permute-done.2 = bf16[256,512]{0,1:T(8,128)(2,1)} collective-permute-done((bf16[256,512]{0,1:T(8,128)(2,1)S(1)}, bf16[256,512]{0,1:T(8,128)(2,1)}, u32[]{:S(2)}, u32[]{:S(2)}) %collective-permute-start.2) | collective-permute-done | bytes 262176 | tf_op jit(solution)/shard_map/ppermute | solution.py:16
  60.5 18.7 %all-gather = s32[8,1,256]{2,1,0:T(1,128)S(1)} all-gather(s32[1,1,256]{2,1,0:T(1,128)} %bitcast.93), channel_id=1, replica_groups=mesh['sp'=8,'tp'=4] {'sp'}, dimensions={0}, use_global_device_ids=true | all-gather | bytes 9216 | tf_op jit(solution)/shard_map/all_gather | solution.py:107
  103.7 6.7 %all-gather.6.cloned.1.call-done = bf16[2048,256]{0,1:T(8,128)(2,1)} async-done(((bf16[256,256]{0,1:T(8,128)(2,1)}), bf16[2048,256]{0,1:T(8,128)(2,1)}) %all-gather.6.cloned.1.call-update) | async-done | bytes 1048592 | tf_op jit(solution)/shard_map/all_gather | solution.py:84
  110.4 13.7 %conditional.2 = (f32[4,256]{1,0:T(4,128)}, f32[4,256]{1,0:T(4,128)}, f32[4,256]{1,0:T(4,128)}, f32[4,256]{1,0:T(4,128)}) conditional(s32[]{:T(128)} %convert_element_type.56, () %tuple.35, (s32[256]{0:T(256)}, s32[2048]{0:T(1024)S(1)}, s32[256]{0:T(256)S(1)}, bf16[2048,256]{0,1:T(8,128)(2,1)}, bf16[256,4,64]{0,2,1:T(8,128)(2,1)S(1)}, ...), branch_computations={%region_1.0_spmd, %region_2.7_spmd} | conditional | flops 571996160 | bytes 50120764 | solution.py:103
  117.9 6.1 %select_reduce_fusion = (f32[4,256]{1,0:T(4,128)}, f32[4,256]{1,0:T(4,128)}) fusion(f32[4,256,2048]{2,1,0:T(8,128)S(1)} %get-tuple-element.293, f32[4,256]{1,0:T(4,128)} %get-tuple-element.309, pred[256,2048]{1,0:T(8,128)(4,1)S(1)} %fusion.2, f32[4,256]{1,0:T(4,128)} %get-tuple-element.307, f32[4,256,2048]{2,1,0:T(8,128)S(1)} %fusion.55), kind=kLoop, calls=%fused_computation.2 | loop fusion | flops 20969472 | bytes 17317888 | tf_op jit(solution)/shard_map/cond/branch_1_fun/reduce_sum | solution.py:97
  124.0 19.7 %conditional.3 = (f32[4,256,128]{1,2,0:T(8,128)}, f32[4,256,1]{1,0,2:T(4,128)S(1)}) conditional(s32[]{:T(128)} %convert_element_type.56, () %tuple.34, (s32[256]{0:T(256)}, s32[2048]{0:T(1024)S(1)}, s32[256]{0:T(256)}, bf16[2048,256]{0,1:T(8,128)(2,1)}, bf16[256,4,64]{0,2,1:T(8,128)(2,1)S(1)}, /*index=5*/f32[4,256]{1,0:T(4,128)}, ...), branch_computations={%region_7.8_spmd, %region_8.10_spmd.clone} | conditional | flops 1098644480 | bytes 31234324 | solution.py:129
  124.0 4.3 %constant_dynamic-slice_fusion = bf16[2048,512]{0,1:T(8,128)(2,1)} fusion(bf16[4096,512]{0,1:T(8,128)(2,1)} %get-tuple-element.240, s32[]{:T(128)S(6)} %select_n.172), kind=kLoop, calls=%fused_computation.22 | loop fusion | bytes 4194308 | tf_op jit(solution)/shard_map/jit(_roll_dynamic)/dynamic_slice | solution.py:20
  128.4 4.5 %fusion.56 = f32[4,256,2048]{2,1,0:T(8,128)} fusion(bf16[256,4,64]{0,2,1:T(8,128)(2,1)S(1)} %get-tuple-element.232, bf16[2048,4,64]{0,2,1:T(8,128)(2,1)S(1)} %bitcast.75), kind=kOutput, calls=%fused_computation.130 | convolution fusion | flops 268435456 | bytes 9568256 | tf_op jit(solution)/shard_map/cond/branch_1_fun/qhd,khd->hqk/dot_general | solution.py:75
  133.4 10.3 %multiply_reduce_fusion = (f32[4,256]{1,0:T(4,128)S(1)}, f32[4,256,128]{1,2,0:T(8,128)}) fusion(bf16[2048,4,128]{0,2,1:T(8,128)(2,1)} %bitcast.77, f32[4,256,2048]{2,1,0:T(8,128)} %fusion.56, bf16[256,4,64]{0,2,1:T(8,128)(2,1)S(1)} %get-tuple-element.236, bf16[2048,4,64]{0,2,1:T(8,128)(2,1)} %bitcast.83, f32[4,256]{1,0:T(4,128)} %get-tuple-element.239, ...), kind=kOutput, calls=%fused_computation.21 | convolution fusion | flops 828636160 | bytes 12734480 | tf_op jit(solution)/shard_map/cond/branch_1_fun/hqk,khv->hqv/dot_general | solution.py:122
  145.0 3.4 convolution_convert_fusion.1
  149.1 34.7 %all-reduce.2.cloned.1.call-done = bf16[256,2048]{1,0:T(8,128)(2,1)} async-done(((bf16[256,2048]{1,0:T(8,128)(2,1)}), bf16[256,2048]{1,0:T(8,128)(2,1)}) %all-reduce.2.cloned.1.call-update) | async-done | bytes 1048592 | tf_op jit(solution)/shard_map/psum | solution.py:137
  187.5 3.3 gather_fusion
  192.8 53.1 %all_to_all.10 = bf16[8,64,2048]{2,1,0:T(8,128)(2,1)S(1)} all-to-all(bf16[8,64,2048]{2,1,0:T(8,128)(2,1)S(1)} %broadcast_select_fusion), channel_id=1, replica_groups=mesh['sp'=8,'tp'=4] {'sp'}, dimensions={0} | all-to-all | bytes 4194304 | tf_op jit(solution)/shard_map/all_to_all | solution.py:161
  249.4 6.3 %convolution_convert_fusion = bf16[512,2048]{1,0:T(8,128)(2,1)} fusion(bf16[1,512,2048]{2,1,0:T(8,128)(2,1)S(1)} %copy-done, bf16[512,2048]{1,0:T(8,128)(2,1)} %bitcast.79, bf16[1,2048,512]{2,1,0:T(8,128)(2,1)} %param.37, f32[512,512]{1,0:T(8,128)} %fusion.16), kind=kOutput, calls=%fused_computation.26 | convolution fusion | flops 2150105088 | bytes 9437184 | tf_op jit(solution)/shard_map/dot_general | solution.py:167
  255.7 4.5 %all-to-all-start.1 = ((bf16[8,64,2048]{2,1,0:T(8,128)(2,1)}), bf16[8,64,2048]{2,1,0:T(8,128)(2,1)}, u32[]{:S(2)}, u32[]{:S(2)}) async-start(bf16[8,64,2048]{2,1,0:T(8,128)(2,1)} %bitcast.76), calls=%async_computation.1 | async-start | bytes 4194304 | tf_op jit(solution)/shard_map/all_to_all | solution.py:170
  262.1 45.3 %all-to-all-done.1 = bf16[8,64,2048]{2,1,0:T(8,128)(2,1)} async-done(((bf16[8,64,2048]{2,1,0:T(8,128)(2,1)}), bf16[8,64,2048]{2,1,0:T(8,128)(2,1)}, u32[]{:S(2)}, u32[]{:S(2)}) %all-to-all-start.1) | async-done | bytes 2097184 | tf_op jit(solution)/shard_map/all_to_all | solution.py:170
  307.4 10.7 %gather_fusion.1 = bf16[1024,2048]{1,0:T(8,128)(2,1)} fusion(bf16[512,2048]{1,0:T(8,128)(2,1)} %bitcast.20, s32[1024]{0:T(1024)S(1)} %broadcast_clamp_fusion), kind=kCustom, calls=%fused_computation.1 | custom fusion | bytes 8392704 | tf_op jit(solution)/shard_map/gather | solution.py:178
  318.1 8.3 %reshape.457 = f32[256,4,2048]{2,1,0:T(4,128)} reshape(bf16[1024,2048]{1,0:T(8,128)(2,1)} %gather_fusion.1) | data formatting | bytes 12582912 | tf_op jit(solution)/shard_map/convert_element_type | solution.py:178
  326.4 11.4 %multiply_reduce_fusion.1 = f32[256,2048]{1,0:T(8,128)} fusion(f32[256,4,2048]{2,1,0:T(4,128)} %reshape.457, f32[256,4]{1,0:T(8,128)S(1)} %copy.68), kind=kLoop, calls=%fused_computation.25 | loop fusion | flops 3670016 | bytes 10489856 | tf_op jit(solution)/shard_map/reduce_sum | solution.py:180
  337.8 3.7 fusion.12
  341.6 23.9 %reduce-scatter.2.cloned.1.call-done = bf16[64,2048]{1,0:T(8,128)(2,1)} async-done(((bf16[256,2048]{1,0:T(8,128)(2,1)}), bf16[64,2048]{1,0:T(8,128)(2,1)}) %reduce-scatter.2.cloned.1.call-update) | async-done | bytes 262160 | tf_op jit(solution)/shard_map/reduce_scatter | solution.py:188
  (116 shorter events, 68.3 us)
Async XLA Ops:
  6.5 242.9 %copy-start = (bf16[1,512,2048]{2,1,0:T(8,128)(2,1)S(1)}, bf16[1,512,2048]{2,1,0:T(8,128)(2,1)}, u32[]{:S(2)}) copy-start(bf16[1,512,2048]{2,1,0:T(8,128)(2,1)} %param.38) | copy-start | bytes 6291460
  6.5 97.1 %all-gather.4.cloned.1.call-start = ((), (), s32[]{:S(2)}) async-start(), calls=%async_computation.3 | async-start | bytes 1179648 | tf_op jit(solution)/shard_map/all_gather | solution.py:104
  8.4 102.0 %all-gather.6.cloned.1.call-start = ((), (), s32[]{:S(2)}) async-start(), calls=%async_computation.4 | async-start | bytes 1179648 | tf_op jit(solution)/shard_map/all_gather | solution.py:84
  9.5 15.6 %collective-permute-start = (bf16[256,512]{0,1:T(8,128)(2,1)S(1)}, bf16[256,512]{0,1:T(8,128)(2,1)S(1)}, u32[]{:S(2)}, u32[]{:S(2)}) collective-permute-start(bf16[256,512]{0,1:T(8,128)(2,1)S(1)} %copy.61), channel_id=1, source_target_pairs={{0,4},{4,8},{8,12},{12,16},{16,20},{20,24},{24,28},{28,0},{1,5},{5... | collective-permute-start | bytes 786440 | tf_op jit(solution)/shard_map/ppermute | solution.py:16
  12.5 27.0 %collective-permute-start.4 = (bf16[256,512]{0,1:T(8,128)(2,1)S(1)}, bf16[256,512]{0,1:T(8,128)(2,1)S(1)}, u32[]{:S(2)}, u32[]{:S(2)}) collective-permute-start(bf16[256,512]{0,1:T(8,128)(2,1)S(1)} %copy.61), channel_id=1, source_target_pairs={{0,28},{4,0},{8,4},{12,8},{16,12},{20,16},{24,20},{28,24},{1,29},{... | collective-permute-start | bytes 786440 | tf_op jit(solution)/shard_map/ppermute | solution.py:18
  17.3 166.5 %all-reduce.2.cloned.1.call-start = ((), (), s32[]{:S(2)}) async-start(), calls=%async_computation.5 | async-start | bytes 2097152 | tf_op jit(solution)/shard_map/psum | solution.py:137
  25.1 13.8 %collective-permute-start.1 = (bf16[256,512]{0,1:T(8,128)(2,1)S(1)}, bf16[256,512]{0,1:T(8,128)(2,1)S(1)}, u32[]{:S(2)}, u32[]{:S(2)}) collective-permute-start(bf16[256,512]{0,1:T(8,128)(2,1)S(1)} %collective-permute-done), channel_id=1, source_target_pairs={{0,4},{4,8},{8,12},{12,16},{16,20},{20,24},{24,28},{28,0},{1,5},{5... | collective-permute-start | bytes 786440 | tf_op jit(solution)/shard_map/ppermute | solution.py:16
  38.9 16.7 %collective-permute-start.2 = (bf16[256,512]{0,1:T(8,128)(2,1)S(1)}, bf16[256,512]{0,1:T(8,128)(2,1)}, u32[]{:S(2)}, u32[]{:S(2)}) collective-permute-start(bf16[256,512]{0,1:T(8,128)(2,1)S(1)} %collective-permute-done.1), channel_id=1, source_target_pairs={{0,4},{4,8},{8,12},{12,16},{16,20},{20,24},{24,28},{28,0},{1,5},{5... | collective-permute-start | bytes 786440 | tf_op jit(solution)/shard_map/ppermute | solution.py:16
  39.5 44.9 %collective-permute-start.5 = (bf16[256,512]{0,1:T(8,128)(2,1)S(1)}, bf16[256,512]{0,1:T(8,128)(2,1)}, u32[]{:S(2)}, u32[]{:S(2)}) collective-permute-start(bf16[256,512]{0,1:T(8,128)(2,1)S(1)} %collective-permute-done.4), channel_id=1, source_target_pairs={{0,28},{4,0},{8,4},{12,8},{16,12},{20,16},{24,20},{28,24},{1,29},{... | collective-permute-start | bytes 786440 | tf_op jit(solution)/shard_map/ppermute | solution.py:18
  55.6 30.5 %collective-permute-start.3 = (bf16[256,512]{0,1:T(8,128)(2,1)}, bf16[256,512]{0,1:T(8,128)(2,1)}, u32[]{:S(2)}, u32[]{:S(2)}) collective-permute-start(bf16[256,512]{0,1:T(8,128)(2,1)} %collective-permute-done.2), channel_id=1, source_target_pairs={{0,4},{4,8},{8,12},{12,16},{16,20},{20,24},{24,28},{28,0},{1,5},{5... | collective-permute-start | bytes 786440 | tf_op jit(solution)/shard_map/ppermute | solution.py:16
  58.2 22.9 %copy-start.13 = (s32[256]{0:T(256)}, s32[256]{0:T(256)S(1)}, u32[]{:S(2)}) copy-start(s32[256]{0:T(256)S(1)} %iota_add_fusion) | copy-start | bytes 3076
  84.4 25.9 %copy-start.10 = (s32[256]{0:T(256)S(1)}, s32[256]{0:T(256)}, u32[]{:S(2)}) copy-start(s32[256]{0:T(256)} %param.29) | copy-start | bytes 3076
  84.4 9.7 %collective-permute-start.6 = (bf16[256,512]{0,1:T(8,128)(2,1)}, bf16[256,512]{0,1:T(8,128)(2,1)S(1)}, u32[]{:S(2)}, u32[]{:S(2)}) collective-permute-start(bf16[256,512]{0,1:T(8,128)(2,1)} %collective-permute-done.5), channel_id=1, source_target_pairs={{0,28},{4,0},{8,4},{12,8},{16,12},{20,16},{24,20},{28,24},{1,29},{... | collective-permute-start | bytes 786440 | tf_op jit(solution)/shard_map/ppermute | solution.py:18
  128.4 4.5 %copy-start.11 = (s32[256]{0:T(256)S(1)}, s32[256]{0:T(256)}, u32[]{:S(2)}) copy-start(s32[256]{0:T(256)} %get-tuple-element.231) | copy-start | bytes 3076 | tf_op jit(solution)/shard_map/cond
  128.4 4.5 %copy-start.14 = (s32[256]{0:T(256)S(1)}, s32[256]{0:T(256)}, u32[]{:S(2)}) copy-start(s32[256]{0:T(256)} %get-tuple-element.229) | copy-start | bytes 3076 | tf_op jit(solution)/shard_map/cond
  143.7 5.1 %copy-start.9 = (s32[1024]{0:T(1024)S(1)}, s32[1024]{0:T(1024)}, u32[]{:S(2)}) copy-start(s32[1024]{0:T(1024)} %get-tuple-element.302) | copy-start | bytes 12292
  143.7 40.1 %copy-start.2 = (bf16[256,2048]{1,0:T(8,128)(2,1)S(1)}, bf16[256,2048]{1,0:T(8,128)(2,1)}, u32[]{:S(2)}) copy-start(bf16[256,2048]{1,0:T(8,128)(2,1)} %param.23) | copy-start | bytes 3145732
  145.0 41.9 %copy-start.12 = (f32[2048]{0:T(1024)S(1)}, f32[2048]{0:T(1024)}, u32[]{:S(2)}) copy-start(f32[2048]{0:T(1024)} %param.33) | copy-start | bytes 24580
  190.8 56.3 %copy-start.16 = (bf16[1,2048,512]{2,1,0:T(8,128)(2,1)S(1)}, bf16[1,2048,512]{2,1,0:T(8,128)(2,1)}, u32[]{:S(2)}) copy-start(bf16[1,2048,512]{2,1,0:T(8,128)(2,1)} %param.36) | copy-start | bytes 6291460
  255.7 4.7 %copy-start.7 = (s32[256,4]{0,1:T(4,128)S(1)}, s32[256,4]{0,1:T(4,128)}, u32[]{:S(2)}) copy-start(s32[256,4]{0,1:T(4,128)} %param.34) | copy-start | bytes 12292
  255.7 4.7 %copy-start.15 = (f32[256,4]{0,1:T(4,128)S(1)}, f32[256,4]{0,1:T(4,128)}, u32[]{:S(2)}) copy-start(f32[256,4]{0,1:T(4,128)} %param.35) | copy-start | bytes 12292
  255.7 4.9 %copy-start.8 = (s32[1024]{0:T(1024)S(1)}, s32[1024]{0:T(1024)}, u32[]{:S(2)}) copy-start(s32[1024]{0:T(1024)} %get-tuple-element.300) | copy-start | bytes 12292
  255.7 51.8 %all-to-all-start.1 = ((bf16[8,64,2048]{2,1,0:T(8,128)(2,1)}), bf16[8,64,2048]{2,1,0:T(8,128)(2,1)}, u32[]{:S(2)}, u32[]{:S(2)}) async-start(bf16[8,64,2048]{2,1,0:T(8,128)(2,1)} %bitcast.76), calls=%async_computation.1 | async-start | bytes 4194304 | tf_op jit(solution)/shard_map/all_to_all | solution.py:170
  260.2 105.3 %reduce-scatter.2.cloned.1.call-start = ((), (), s32[]{:S(2)}) async-start(), calls=%async_computation.6 | async-start | bytes 1310720 | tf_op jit(solution)/shard_map/reduce_scatter | solution.py:188
  (5 other events, 14.4 us)
Sparse Core Ops, SparseCore 0:
  9.4 56.0 all-gather.3
  67.5 42.8 all-gather.5
  148.5 35.2 all-reduce.1
  341.7 23.7 reduce-scatter.1
